TPU v7x, 32 devices: a whole 2x2x4 slice. The times are simulated.
32 devices in a mesh: gr: 2 (over y), fs: 4 (over z), tp: 4 (over x, core).
Axes of the slice: x: 2, y: 2, z: 4, core: 2. Of those that a mesh axis runs over, the one named last changes fastest.
Arguments:
- prompt: bfloat16 [4096, 2048], P(('gr', 'fs')), may hold values from -6 to 6
- norm_gain: float32 [2048], P(('gr', 'fs')), may hold values from 0.1 to 1.9
- gate_master: float32 [32, 2048, 1024], P(None, ('gr', 'fs'), 'tp'), may hold values from -6 to 6
- up_master: float32 [32, 2048, 1024], P(None, ('gr', 'fs'), 'tp'), may hold values from -6 to 6
- down_master: float32 [32, 2048, 1024], P(None, ('gr', 'fs'), 'tp'), may hold values from -6 to 6
- routes: int32 [4096, 2], P(('gr', 'fs')), may hold values from 0 to 31, as said below
- route_weights: float32 [4096, 2], P(('gr', 'fs')), may hold values from 0.1 to 0.9
Outputs:
- gate_ready: bfloat16 [32, 2048, 1024], P('fs', None, 'tp')
- up_ready: bfloat16 [32, 2048, 1024], P('fs', None, 'tp')
- down_ready: bfloat16 [32, 2048, 1024], P('fs', None, 'tp')
- blended: bfloat16 [4096, 2048], P(('gr', 'fs'), 'tp')
Inputs may be any that keep to these rules, and one draw needn't show every extreme that they name: `routes`: each row names 2 different experts of one group: expert // 8 is the group. In every aligned block of 512 rows (the tokens of one index of gr and fs) half of the rows choose one group, and no expert is named more than 64 times; in every block some expert is named exactly 64 times.
All inputs are finite; a program needn't handle non-finite values.
Results may differ from a plain program's by a relative error of at most 0.015.
Values may be sent and summed in bfloat16 or wider, within the bound.
A program may use at most 128 MiB of HBM per device.

v0:
```python
import jax
import jax.numpy as jnp
from jax import lax
from jax.sharding import PartitionSpec as P

D = 2048
FF = 1024


EPS = 1e-06


def per_device(prompt, norm_gain, gate_master, up_master, down_master, routes, route_weights):
    gate_low = (norm_gain[None, :, None] * gate_master).astype(jnp.bfloat16)
    up_low = (norm_gain[None, :, None] * up_master).astype(jnp.bfloat16)
    down_low = down_master.astype(jnp.bfloat16)
    experts = gate_low.shape[0]
    fs_count = lax.axis_size("fs")
    local_experts = experts // fs_count
    resharded = (
        lax.all_to_all(gate_low, "fs", split_axis=0, concat_axis=1, tiled=True),
        lax.all_to_all(up_low, "fs", split_axis=0, concat_axis=1, tiled=True),
        lax.all_to_all(down_low, "fs", split_axis=0, concat_axis=1, tiled=True),
    )
    gate_ready, up_ready, down_ready = (
        lax.all_gather(resharded[0], "gr", axis=1, tiled=True),
        lax.all_gather(resharded[1], "gr", axis=1, tiled=True),
        lax.all_gather(resharded[2], "gr", axis=1, tiled=True),
    )
    tokens = prompt.shape[0]
    capacity = tokens // 8
    prompt_wide = prompt.astype(jnp.float32)
    normed = (
        prompt_wide * lax.rsqrt(jnp.mean(prompt_wide * prompt_wide, axis=-1, keepdims=True) + EPS)
    ).astype(jnp.bfloat16)
    route_list = routes.reshape(-1)
    route_hits = (route_list[:, None] == jnp.arange(experts, dtype=jnp.int32)[None, :]).astype(
        jnp.int32
    )
    slot_rank = jnp.sum((jnp.cumsum(route_hits, axis=0) - 1) * route_hits, axis=1)
    slot_index = route_list * capacity + slot_rank
    token_of = jnp.arange(route_list.shape[0], dtype=jnp.int32) // routes.shape[1]
    slot_owner = jnp.zeros((experts * capacity,), jnp.int32).at[slot_index].set(token_of)
    outgoing = normed[slot_owner].reshape(fs_count, local_experts, capacity, normed.shape[1])
    arrived = lax.all_to_all(outgoing, "fs", split_axis=0, concat_axis=0, tiled=True)
    pre_gate = jnp.einsum(
        "secd,edf->secf", arrived, gate_ready, preferred_element_type=jnp.float32
    ) * D ** (-0.5)
    pre_up = jnp.einsum(
        "secd,edf->secf", arrived, up_ready, preferred_element_type=jnp.float32
    ) * D ** (-0.5)
    hidden = (jax.nn.silu(pre_gate) * pre_up).astype(jnp.bfloat16)
    partial_value = (
        jnp.einsum("secf,edf->secd", hidden, down_ready, preferred_element_type=jnp.float32)
        * FF ** (-0.5)
    ).astype(jnp.bfloat16)
    summed = lax.psum_scatter(partial_value, "tp", scatter_dimension=3, tiled=True).astype(
        jnp.float32
    )
    answers = lax.all_to_all(
        summed.astype(jnp.bfloat16), "fs", split_axis=0, concat_axis=0, tiled=True
    )
    answers_flat = answers.reshape(experts * capacity, answers.shape[3])
    picked = answers_flat[slot_index].reshape(tokens, routes.shape[1], answers.shape[3])
    blended = jnp.sum(picked.astype(jnp.float32) * route_weights[:, :, None], axis=1)
    return (gate_ready, up_ready, down_ready, blended.astype(jnp.bfloat16))


def solution(mesh):
    in_specs = (
        P(("gr", "fs"), None),
        P(("gr", "fs")),
        P(None, ("gr", "fs"), "tp"),
        P(None, ("gr", "fs"), "tp"),
        P(None, ("gr", "fs"), "tp"),
        P(("gr", "fs"), None),
        P(("gr", "fs"), None),
    )
    out_specs = (
        P("fs", None, "tp"),
        P("fs", None, "tp"),
        P("fs", None, "tp"),
        P(("gr", "fs"), "tp"),
    )
    return jax.shard_map(
        per_device, mesh=mesh, in_specs=in_specs, out_specs=out_specs, check_vma=False
    )
```

profile of v0, /device:TPU:20, one launch (start us, length us, event | category | flops | bytes accessed | tf_op | source)
XLA Modules:
  0.0 687.3 jit_solution(8240424116408428662)
XLA Ops:
  7.2 11.5 %multiply_convert_fusion.1 = (bf16[32,256,256]{2,1,0:T(8,128)(2,1)}, bf16[32,256,256]{2,1,0:T(8,128)(2,1)}) fusion(f32[32,256,256]{2,1,0:T(8,128)} %param.10, f32[256]{0:T(256)} %param.8, f32[32,256,256]{2,1,0:T(8,128)} %param.9), kind=kLoop, calls=%fused_computation.11 | loop fusion | flops 8388608 | bytes 25166848 | tf_op jit(solution)/shard_map/convert_element_type | solution.py:15
  18.7 96.7 %all_to_all.64 = bf16[32,256,256]{2,1,0:T(8,128)(2,1)} all-to-all(bf16[32,256,256]{2,1,0:T(8,128)(2,1)} %get-tuple-element.4), channel_id=1, replica_groups=mesh['gr'=2,'fs'=4,'tp'=4] {'fs'}, dimensions={0} | all-to-all | bytes 8388608 | tf_op jit(solution)/shard_map/all_to_all | solution.py:22
  115.4 7.6 %all-to-all-start = ((bf16[32,256,256]{2,1,0:T(8,128)(2,1)}), bf16[32,256,256]{2,1,0:T(8,128)(2,1)}, u32[]{:S(2)}, u32[]{:S(2)}) async-start(bf16[32,256,256]{2,1,0:T(8,128)(2,1)} %get-tuple-element.5), calls=%async_computation | async-start | bytes 8388608 | tf_op jit(solution)/shard_map/all_to_all | solution.py:21
  123.0 4.6 copy.27
  127.7 5.9 convert_element_type.42
  133.6 78.5 %all-to-all-done = bf16[32,256,256]{2,1,0:T(8,128)(2,1)} async-done(((bf16[32,256,256]{2,1,0:T(8,128)(2,1)}), bf16[32,256,256]{2,1,0:T(8,128)(2,1)}, u32[]{:S(2)}, u32[]{:S(2)}) %all-to-all-start) | async-done | bytes 4194336 | tf_op jit(solution)/shard_map/all_to_all | solution.py:21
  212.1 8.2 %all-to-all-start.2 = ((bf16[32,256,256]{2,1,0:T(8,128)(2,1)}), bf16[32,256,256]{2,1,0:T(8,128)(2,1)}, u32[]{:S(2)}, u32[]{:S(2)}) async-start(bf16[32,256,256]{2,1,0:T(8,128)(2,1)} %convert_element_type.42), calls=%async_computation.2 | async-start | bytes 8388608 | tf_op jit(solution)/shard_map/all_to_all | solution.py:23
  220.2 4.6 copy.26
  224.9 0.7 copy-done.1
  226.1 9.0 %reduce-window.6 = s32[32,8,128]{2,1,0:T(8,128)S(1)} reduce-window(s32[32,8,128]{2,1,0:T(8,128)S(1)} %fusion.29, s32[]{:T(128)} %constant.36.clone.1), window={size=1x1x128 pad=0_0x0_0x127_0}, to_apply=%region_1.0 | reduce-window | flops 4161536 | bytes 262148 | tf_op jit(solution)/shard_map/reduce-window
  235.6 0.2 mul.86
  236.0 4.3 scatter_custom_fusion
  240.3 0.5 fusion.9
  240.8 2.3 fusion.10
  243.1 10.9 %gather_fusion = bf16[2048,2048]{1,0:T(8,128)(2,1)} fusion(bf16[512,2048]{1,0:T(8,128)(2,1)S(1)} %fusion.10, s32[2048]{0:T(1024)S(1)} %fusion.30), kind=kCustom, calls=%fused_computation | custom fusion | bytes 16785408 | tf_op jit(solution)/shard_map/gather | solution.py:44
  254.0 55.7 %all-to-all-done.2 = bf16[32,256,256]{2,1,0:T(8,128)(2,1)} async-done(((bf16[32,256,256]{2,1,0:T(8,128)(2,1)}), bf16[32,256,256]{2,1,0:T(8,128)(2,1)}, u32[]{:S(2)}, u32[]{:S(2)}) %all-to-all-start.2) | async-done | bytes 4194336 | tf_op jit(solution)/shard_map/all_to_all | solution.py:23
  309.7 9.0 %all-to-all-start.3 = ((bf16[4,8,64,2048]{3,2,1,0:T(8,128)(2,1)}), bf16[4,8,64,2048]{3,2,1,0:T(8,128)(2,1)}, u32[]{:S(2)}, u32[]{:S(2)}) async-start(bf16[4,8,64,2048]{3,2,1,0:T(8,128)(2,1)} %bitcast.75), calls=%async_computation.3 | async-start | bytes 16777216 | tf_op jit(solution)/shard_map/all_to_all | solution.py:45
  318.7 4.7 copy.28
  323.4 0.2 reduce-scatter.2.cloned.1.call-start
  323.6 174.4 %all-to-all-done.3 = bf16[4,8,64,2048]{3,2,1,0:T(8,128)(2,1)} async-done(((bf16[4,8,64,2048]{3,2,1,0:T(8,128)(2,1)}), bf16[4,8,64,2048]{3,2,1,0:T(8,128)(2,1)}, u32[]{:S(2)}, u32[]{:S(2)}) %all-to-all-start.3) | async-done | bytes 8388640 | tf_op jit(solution)/shard_map/all_to_all | solution.py:45
  498.0 8.1 %fusion.3 = f32[8,256,4,64]{1,3,2,0:T(8,128)S(1)} fusion(bf16[8,2048,256]{2,1,0:T(8,128)(2,1)} %all-gather.6.cloned.1.call-done, bf16[4,8,64,2048]{3,2,1,0:T(8,128)(2,1)} %all-to-all-done.3), kind=kOutput, calls=%fused_computation.7 | convolution fusion | flops 2147483648 | bytes 18874368 | tf_op jit(solution)/shard_map/secd,edf->secf/dot_general | solution.py:49
  506.1 17.0 %fusion = bf16[4,8,64,2048]{3,2,0,1:T(8,128)(2,1)} fusion(bf16[8,2048,256]{2,1,0:T(8,128)(2,1)} %all-gather.8.cloned.1.call-done, f32[8,256,4,64]{1,3,2,0:T(8,128)S(1)} %fusion.3, bf16[4,8,64,2048]{3,2,1,0:T(8,128)(2,1)} %all-to-all-done.3, bf16[8,2048,256]{2,1,0:T(8,128)(2,1)} %all-gather.4.cloned.1.call-done), kind=kOutput, calls=%fused_computation.4 | convolution fusion | flops 4307550208 | bytes 35651584 | tf_op jit(solution)/shard_map/secf,edf->secd/dot_general | solution.py:54
  523.2 73.3 %reduce-scatter.2.cloned.1.call-done = bf16[4,8,64,512]{3,2,0,1:T(8,128)(2,1)} async-done(((bf16[4,8,64,2048]{3,2,0,1:T(8,128)(2,1)}), bf16[4,8,64,512]{3,2,0,1:T(8,128)(2,1)}) %reduce-scatter.2.cloned.1.call-update) | async-done | bytes 2097168 | tf_op jit(solution)/shard_map/reduce_scatter | solution.py:57
  596.5 3.1 copy.36
  599.6 5.1 all-to-all-start.4
  604.9 44.6 %all-to-all-done.4 = bf16[4,8,64,512]{3,2,1,0:T(8,128)(2,1)S(1)} async-done(((bf16[4,8,64,512]{3,2,1,0:T(8,128)(2,1)}), bf16[4,8,64,512]{3,2,1,0:T(8,128)(2,1)S(1)}, u32[]{:S(2)}, u32[]{:S(2)}) %all-to-all-start.4) | async-done | bytes 2097184 | tf_op jit(solution)/shard_map/all_to_all | solution.py:60
  649.5 4.0 gather_fusion.1
  653.5 1.3 reshape.78
  654.8 4.0 multiply_reduce_fusion
  658.8 7.3 %copy.54 = bf16[8,2048,256]{2,1,0:T(8,128)(2,1)} copy(bf16[8,2048,256]{2,1,0:T(8,128)(2,1)} %all-gather.4.cloned.1.call-done) | data formatting | bytes 16777216
  666.2 7.3 %copy.55 = bf16[8,2048,256]{2,1,0:T(8,128)(2,1)} copy(bf16[8,2048,256]{2,1,0:T(8,128)(2,1)} %all-gather.6.cloned.1.call-done) | data formatting | bytes 16777216
  673.5 7.3 %copy.56 = bf16[8,2048,256]{2,1,0:T(8,128)(2,1)} copy(bf16[8,2048,256]{2,1,0:T(8,128)(2,1)} %all-gather.8.cloned.1.call-done) | data formatting | bytes 16777216
  (34 shorter events, 1.4 us)
Async XLA Ops:
  115.4 96.7 %all-to-all-start = ((bf16[32,256,256]{2,1,0:T(8,128)(2,1)}), bf16[32,256,256]{2,1,0:T(8,128)(2,1)}, u32[]{:S(2)}, u32[]{:S(2)}) async-start(bf16[32,256,256]{2,1,0:T(8,128)(2,1)} %get-tuple-element.5), calls=%async_computation | async-start | bytes 8388608 | tf_op jit(solution)/shard_map/all_to_all | solution.py:21
  123.0 375.0 %all-gather.6.cloned.1.call-start = ((), (), s32[]{:S(2)}) async-start(), calls=%async_computation.7 | async-start | bytes 12582912 | tf_op jit(solution)/shard_map/all_gather | solution.py:27
  212.1 97.6 %all-to-all-start.2 = ((bf16[32,256,256]{2,1,0:T(8,128)(2,1)}), bf16[32,256,256]{2,1,0:T(8,128)(2,1)}, u32[]{:S(2)}, u32[]{:S(2)}) async-start(bf16[32,256,256]{2,1,0:T(8,128)(2,1)} %convert_element_type.42), calls=%async_computation.2 | async-start | bytes 8388608 | tf_op jit(solution)/shard_map/all_to_all | solution.py:23
  220.2 285.8 %all-gather.4.cloned.1.call-start = ((), (), s32[]{:S(2)}) async-start(), calls=%async_computation.6 | async-start | bytes 12582912 | tf_op jit(solution)/shard_map/all_gather | solution.py:26
  224.9 0.7 copy-start.1
  224.9 15.4 %copy-start = (bf16[512,2048]{1,0:T(8,128)(2,1)S(1)}, bf16[512,2048]{1,0:T(8,128)(2,1)}, u32[]{:S(2)}) copy-start(bf16[512,2048]{1,0:T(8,128)(2,1)} %param.7) | copy-start | bytes 6291460
  309.7 188.3 %all-to-all-start.3 = ((bf16[4,8,64,2048]{3,2,1,0:T(8,128)(2,1)}), bf16[4,8,64,2048]{3,2,1,0:T(8,128)(2,1)}, u32[]{:S(2)}, u32[]{:S(2)}) async-start(bf16[4,8,64,2048]{3,2,1,0:T(8,128)(2,1)} %bitcast.75), calls=%async_computation.3 | async-start | bytes 16777216 | tf_op jit(solution)/shard_map/all_to_all | solution.py:45
  318.7 187.5 %all-gather.8.cloned.1.call-start = ((), (), s32[]{:S(2)}) async-start(), calls=%async_computation.8 | async-start | bytes 12582912 | tf_op jit(solution)/shard_map/all_gather | solution.py:28
  323.4 273.1 %reduce-scatter.2.cloned.1.call-start = ((), (), s32[]{:S(2)}) async-start(), calls=%async_computation.9 | async-start | bytes 10485760 | tf_op jit(solution)/shard_map/reduce_scatter | solution.py:57
  523.2 81.5 %copy-start.2 = (f32[512,2]{0,1:T(2,128)S(1)}, f32[512,2]{0,1:T(2,128)}, u32[]{:S(2)}) copy-start(f32[512,2]{0,1:T(2,128)} %param.13) | copy-start | bytes 12292
  599.6 49.9 %all-to-all-start.4 = ((bf16[4,8,64,512]{3,2,1,0:T(8,128)(2,1)}), bf16[4,8,64,512]{3,2,1,0:T(8,128)(2,1)S(1)}, u32[]{:S(2)}, u32[]{:S(2)}) async-start(bf16[4,8,64,512]{3,2,1,0:T(8,128)(2,1)} %copy.36), calls=%async_computation.5 | async-start | bytes 4194304 | tf_op jit(solution)/shard_map/all_to_all | solution.py:60
Sparse Core Ops, SparseCore 0:
  127.8 103.9 all-gather.5
  233.9 103.9 all-gather.3
  339.5 103.9 all-gather.7
  523.3 73.1 reduce-scatter.1
where the time goes:
time: 693 us; the launch traced here: 687 us
  waiting for transfers between devices  427 us (62%)
  blocking collectives  96.7 us (14%)
  local copies, waits for them, and re-layouts  61.4 us (9%)
  other arithmetic  33.5 us (5%)
  starting transfers between devices  30.1 us (4%)
  matrix products  25.1 us (4%)
  between operations  13.9 us (2%)
    all_to_all x1, waiting for transfers between devices, per_device(): lax.all_to_all(outgoing, 'fs', split_axis=0, concat_axis=0, tiled=True)  174 us
    all_to_all x1, blocking collectives, per_device(): lax.all_to_all(up_low, 'fs', split_axis=0, concat_axis=1, tiled=True)  96.7 us
    all_to_all x1, waiting for transfers between devices, per_device(): lax.all_to_all(gate_low, 'fs', split_axis=0, concat_axis=1, tiled=True)  78.5 us
    reduce_scatter x1, waiting for transfers between devices, per_device(): lax.psum_scatter(partial_value, 'tp', scatter_dimension=3, tiled=True)  73.3 us
    all_to_all x1, waiting for transfers between devices, per_device(): lax.all_to_all(down_low, 'fs', split_axis=0, concat_axis=1, tiled=True)  55.7 us
    all_to_all x1, waiting for transfers between devices, per_device(): lax.all_to_all(summed.astype(jnp.bfloat16), 'fs', split_axis=0, concat_ax...  44.6 us
    unnamed x11, local copies, waits for them, and re-layouts  22.9 us
    dot_general x1, matrix products, per_device(): jnp.einsum('secf,edf->secd', hidden, down_ready, preferred_element_type=j...  17 us
  transfers between devices with their start and end apart: 8, of which 5 were waited for; matrix products, arithmetic and copies ran while one was open for 8% of the time, Pallas kernels for 0%

commit v1 on v0

v1 whole, which is shorter than its diff:
```python
import functools

import jax
import jax.numpy as jnp
from jax import lax
from jax.experimental import pallas as pl
from jax.experimental.pallas import tpu as pltpu
from jax.sharding import PartitionSpec as P

EPS = 1e-06
GROUP = 8
MESH = pl.DeviceIdType.MESH
STEPS = ((0, 0), (1, 0), (0, 1), (1, 1), (2, 0), (2, 1))
SLOTS = 4


def kernel(
    dims, gain, gm, um, dm, tok, wsend, g_out, u_out, d_out, ans,
    stage, wb, x, w, gb, ub, db, hid, yr, ys,
    st_sem, zs, zr, vs, vr, own_sem, tzs, tzr, wzs, wzr, txs, txr, tw_sem, ld_sem, dl_sem,
    ps, pr, rs, rr, rl_sem,
):
    gr, fs, tp, experts, rows, width, cap, depth, hidden_all = dims
    me_g, me_f, me_t = lax.axis_index("gr"), lax.axis_index("fs"), lax.axis_index("tp")
    local = experts // fs
    half = local // 2
    quarter = depth // tp
    total = fs * cap
    tile = min(256, cap)
    piece_rows = max(rows, 128)
    per_owner = quarter // piece_rows
    masters, outs = (gm, um, dm), (g_out, u_out, d_out)

    def fs_at(k):
        return lax.rem(me_f + k, fs)

    def fs_from(k):
        return lax.rem(me_f + fs - k, fs)

    def gr_at(j):
        return lax.rem(me_g + j, gr)

    def remote(src, dst, ssem, rsem, where):
        return pltpu.make_async_remote_copy(
            src_ref=src, dst_ref=dst, send_sem=ssem, recv_sem=rsem,
            device_id=where, device_id_type=MESH,
        )

    def region(s, g, f):
        m, h = STEPS[s]
        at = pl.multiple_of((g * fs + f) * rows, rows)
        return outs[m].at[pl.ds(h * half, half), pl.ds(at, rows), :]

    barrier = pltpu.get_barrier_semaphore()
    for k in range(1, fs):
        pl.semaphore_signal(barrier, inc=1, device_id={"fs": fs_at(k)}, device_id_type=MESH)
    for j in range(1, gr):
        pl.semaphore_signal(barrier, inc=1, device_id={"gr": gr_at(j)}, device_id_type=MESH)
    for j in range(1, tp):
        pl.semaphore_signal(
            barrier, inc=1, device_id={"tp": lax.rem(me_t + j, tp)}, device_id_type=MESH
        )
    pl.semaphore_wait(barrier, (fs - 1) + (gr - 1) + (tp - 1))

    def x_block(f, t):
        return x.at[
            pl.ds(pl.multiple_of(f * cap, cap), cap),
            pl.ds(pl.multiple_of(t * quarter, quarter), quarter),
        ]

    def w_block(f):
        return w.at[pl.ds(pl.multiple_of(f * cap, cap), cap), :]

    items = [(s, k) for s in range(len(STEPS)) for k in range(fs)]

    def load(i):
        s, k = items[i]
        m, h = STEPS[s]
        return pltpu.make_async_copy(
            masters[m].at[pl.ds(fs_at(k) * local + h * half, half)],
            stage.at[i % SLOTS], st_sem.at[i % SLOTS],
        )

    for i in range(SLOTS):
        load(i).start()

    sends = []
    early = []
    for k in range(1, fs):
        dst = fs_at(k)
        c = remote(tok.at[(dst * local) // GROUP], x_block(me_f, me_t), tzs.at[k], tzr.at[k], {"fs": dst})
        c.start()
        sends.append(c)
        c = remote(wsend.at[dst], w_block(me_f), wzs.at[k], wzr.at[k], {"fs": dst})
        c.start()
        sends.append(c)
    own_tok = pltpu.make_async_copy(
        tok.at[(me_f * local) // GROUP], x_block(me_f, me_t), tw_sem.at[0]
    )
    own_tok.start()
    own_w = pltpu.make_async_copy(wsend.at[me_f], w_block(me_f), tw_sem.at[1])
    own_w.start()

    own_copies = {}

    def send_gr(s, k, src):
        f = fs_from(k)
        for j in range(1, gr):
            c = remote(src, region(s, me_g, f), vs.at[s, k, j - 1], vr.at[s, k, j - 1], {"gr": gr_at(j)})
            c.start()
            sends.append(c)

    for i, (s, k) in enumerate(items):
        m, h = STEPS[s]
        load(i).wait()

        def cast(e, carry, s=s, k=k, m=m, i=i):
            value = stage[i % SLOTS, e]
            if m < 2:
                value = gain[...] * value
            wb[s, k, e] = value.astype(jnp.bfloat16)
            return carry

        lax.fori_loop(0, half, cast, 0)
        if i + SLOTS < len(items):
            load(i + SLOTS).start()
        if k == 0:
            c = pltpu.make_async_copy(wb.at[s, 0], region(s, me_g, me_f), own_sem.at[s])
            c.start()
            own_copies[s] = c
            if m < 2:
                send_gr(s, 0, wb.at[s, 0])
        else:
            c = remote(wb.at[s, k], region(s, me_g, me_f), zs.at[s, k], zr.at[s, k], {"fs": fs_at(k)})
            c.start()
            sends.append(c)

    own_tok.wait()
    own_w.wait()
    for k in range(fs):
        f = fs_from(k)
        if k > 0:
            remote(x_block(f, me_t), x_block(f, me_t), tzs.at[k], tzr.at[k], {"fs": f}).wait_recv()
            remote(w_block(f), w_block(f), wzs.at[k], wzr.at[k], {"fs": f}).wait_recv()
        for j in range(1, tp):
            c = remote(
                x_block(f, me_t), x_block(f, me_t), txs.at[k, j], txr.at[k, j],
                {"tp": lax.rem(me_t + j, tp)},
            )
            c.start()
            early.append(c)

    def forward(s, k):
        f = fs_from(k)
        remote(region(s, me_g, f), region(s, me_g, f), zs.at[s, k], zr.at[s, k], {"fs": f}).wait_recv()
        send_gr(s, k, region(s, me_g, f))

    def arrived_gr(s, k):
        f = fs_from(k)
        for j in range(1, gr):
            g = lax.rem(me_g + gr - j, gr)
            remote(
                region(s, g, f), region(s, g, f), vs.at[s, k, j - 1], vr.at[s, k, j - 1], {"gr": g}
            ).wait_recv()

    def loads(e, slot):
        return (
            pltpu.make_async_copy(g_out.at[e], gb.at[slot], ld_sem.at[0, slot]),
            pltpu.make_async_copy(u_out.at[e], ub.at[slot], ld_sem.at[1, slot]),
        )

    def experts_of(h):
        first = h * half
        for c in loads(first, 0):
            c.start()

        def one(n, carry):
            slot = lax.rem(n, 2)
            e = first + n

            @pl.when(n + 1 < half)
            def _():
                for c in loads(e + 1, 1 - slot):
                    c.start()

            for c in loads(e, slot):
                c.wait()

            def block(r, carry):
                at = pl.ds(pl.multiple_of(r * tile, tile), tile)
                xs = x[at, :]
                pre_gate = jnp.dot(xs, gb[slot], preferred_element_type=jnp.float32) * depth ** (-0.5)
                pre_up = jnp.dot(xs, ub[slot], preferred_element_type=jnp.float32) * depth ** (-0.5)
                ws = w[at, :]
                lane = lax.broadcasted_iota(jnp.int32, ws.shape, 1)
                weight = jnp.sum(jnp.where(lane == e, ws, 0.0), axis=1, keepdims=True)
                value = pre_gate / (1.0 + jnp.exp(-pre_gate)) * pre_up * weight
                hid[e, at, :] = value.astype(jnp.bfloat16)
                return carry

            lax.fori_loop(0, total // tile, block, 0)
            return carry

        lax.fori_loop(0, half, one, 0)

    chunks = []

    def chunk(index):
        ci = len(chunks)
        at = pl.multiple_of(index * piece_rows, piece_rows)
        owner = index // per_owner
        piece = lax.rem(index, per_owner)
        slot = ci % 2
        c = pltpu.make_async_copy(d_out.at[:, pl.ds(at, piece_rows), :], db.at[slot], dl_sem.at[slot])
        c.start()
        c.wait()

        def block(r, carry):
            here = pl.ds(pl.multiple_of(r * tile, tile), tile)
            acc = jnp.zeros((tile, piece_rows), jnp.float32)
            for e in range(local):
                acc += lax.dot_general(
                    hid[e, here, :], db[slot, e], (((1,), (1,)), ((), ())),
                    preferred_element_type=jnp.float32,
                )
            x[here, pl.ds(at, piece_rows)] = (acc * hidden_all ** (-0.5)).astype(jnp.bfloat16)
            return carry

        lax.fori_loop(0, total // tile, block, 0)
        turn = lax.rem(me_t + tp - owner, tp)
        slot_of = lax.rem(turn + tp - 1, tp)
        away = turn != 0
        chunks.append((at, owner, piece, slot_of, away))

        @pl.when(away)
        def _():
            partial_copy(ci).start()

    def partial_copy(ci):
        at, owner, piece, slot_of, away = chunks[ci]
        return remote(
            x.at[:, pl.ds(at, piece_rows)],
            yr.at[slot_of, :, pl.ds(pl.multiple_of(piece * piece_rows, piece_rows), piece_rows)],
            ps.at[ci], pr.at[slot_of, piece], {"tp": owner},
        )

    for s in (0, 1, 2):
        for k in range(1, fs):
            forward(s, k)
    send_gr(4, 0, wb.at[4, 0])
    for k in range(fs):
        f = fs_from(k)
        for j in range(1, tp):
            t = lax.rem(me_t + tp - j, tp)
            remote(x_block(f, t), x_block(f, t), txs.at[k, j], txr.at[k, j], {"tp": t}).wait_recv()
    for s in (0, 1):
        own_copies[s].wait()
        for k in range(fs):
            arrived_gr(s, k)
    experts_of(0)
    for k in range(1, fs):
        forward(3, k)
    send_gr(5, 0, wb.at[5, 0])
    for s in (2, 3):
        own_copies[s].wait()
        for k in range(fs):
            arrived_gr(s, k)
    experts_of(1)
    for c in early:
        c.wait_send()
    own_copies[4].wait()
    own_copies[5].wait()
    apart = rows == piece_rows
    if apart:
        chunk(me_g * fs + me_f)
    for k in range(1, fs):
        forward(4, k)
        forward(5, k)
        if apart:
            chunk(me_g * fs + fs_from(k))
    for k in range(fs):
        arrived_gr(4, k)
        arrived_gr(5, k)
        for j in range(1, gr):
            if apart:
                chunk(lax.rem(me_g + gr - j, gr) * fs + fs_from(k))
    if not apart:
        for index in range(depth // piece_rows):
            chunk(jnp.int32(index))

    for j in range(1, tp):
        for p in range(per_owner):
            ref = yr.at[j - 1, :, pl.ds(p * piece_rows, piece_rows)]
            remote(
                ref, ref, rl_sem.at[1], pr.at[j - 1, p], {"tp": lax.rem(me_t + j, tp)}
            ).wait_recv()
    for k in list(range(1, fs)) + [0]:
        f = fs_at(k)
        at = pl.ds(pl.multiple_of(f * cap, cap), cap)
        value = x[at, pl.ds(pl.multiple_of(me_t * quarter, quarter), quarter)].astype(jnp.float32)
        for j in range(tp - 1):
            value += yr[j, at, :].astype(jnp.float32)
        ys[at, :] = value.astype(jnp.bfloat16)
        if k > 0:
            c = remote(ys.at[at, :], ans.at[me_f], rs.at[k], rr.at[k], {"fs": f})
            c.start()
            sends.append(c)
        else:
            own_ans = pltpu.make_async_copy(ys.at[at, :], ans.at[me_f], rl_sem.at[0])
            own_ans.start()
    for k in range(1, fs):
        f = fs_from(k)
        remote(ans.at[f], ans.at[f], rs.at[k], rr.at[k], {"fs": f}).wait_recv()
    own_ans.wait()
    for c in sends:
        c.wait_send()
    for ci in range(len(chunks)):
        @pl.when(chunks[ci][4])
        def _(ci=ci):
            partial_copy(ci).wait_send()


def per_device(prompt, norm_gain, gate_master, up_master, down_master, routes, route_weights):
    gr, fs, tp = lax.axis_size("gr"), lax.axis_size("fs"), lax.axis_size("tp")
    experts, rows, width = gate_master.shape
    tokens, depth = prompt.shape
    local = experts // fs
    half = local // 2
    groups = experts // GROUP
    cap = tokens // 2
    quarter = depth // tp
    total = fs * cap
    piece_rows = max(rows, 128)
    per_owner = quarter // piece_rows
    bf16, f32 = jnp.bfloat16, jnp.float32

    wide = prompt.astype(f32)
    scale = lax.rsqrt(jnp.mean(wide * wide, axis=-1, keepdims=True) + EPS)
    mine = lax.dynamic_slice_in_dim(prompt, lax.axis_index("tp") * quarter, quarter, 1)
    normed = (mine.astype(f32) * scale).astype(bf16)
    group = routes[:, 0] // GROUP
    hits = group[:, None] == jnp.arange(groups, dtype=jnp.int32)[None, :]
    order = jnp.arange(tokens, dtype=jnp.int32)
    before = (order[None, :] < order[:, None]).astype(bf16)
    counts = jnp.dot(before, hits.astype(bf16), preferred_element_type=f32)
    rank = jnp.sum(jnp.where(hits, counts, 0.0), axis=1).astype(jnp.int32)
    slot = group * cap + rank
    place = jnp.arange(groups * cap, dtype=jnp.int32)[:, None] == slot[None, :]
    packed = jnp.dot(place.astype(bf16), normed, preferred_element_type=f32).astype(bf16)
    packed = packed.reshape(groups, cap, quarter)
    named = jnp.arange(experts, dtype=jnp.int32)
    weights = jnp.sum(
        jnp.where(routes[:, :, None] == named[None, None, :], route_weights[:, :, None], 0.0), axis=1
    )
    packed_w = jnp.dot(place.astype(f32), weights, precision=lax.Precision.HIGHEST)
    packed_w = packed_w.reshape(groups, cap, experts)
    sent_w = jnp.stack(
        [
            jnp.pad(
                packed_w[(d * local) // GROUP, :, d * local : (d + 1) * local],
                ((0, 0), (0, 128 - local)),
            )
            for d in range(fs)
        ]
    )
    dims = (gr, fs, tp, experts, rows, width, cap, depth, width * tp)
    any_spec = pl.BlockSpec(memory_space=pl.ANY)
    ready = jax.ShapeDtypeStruct((local, gr * fs * rows, width), bf16)
    steps = len(STEPS)
    dma = pltpu.SemaphoreType.DMA
    gate_ready, up_ready, down_ready, answers = pl.pallas_call(
        functools.partial(kernel, dims),
        name="reshard_experts",
        out_shape=(ready, ready, ready, jax.ShapeDtypeStruct((fs, cap, quarter), bf16)),
        in_specs=[pl.BlockSpec(memory_space=pltpu.VMEM)] + [any_spec] * 5,
        out_specs=(any_spec,) * 4,
        scratch_shapes=[
            pltpu.VMEM((SLOTS, half, rows, width), f32),
            pltpu.VMEM((steps, fs, half, rows, width), bf16),
            pltpu.VMEM((total, depth), bf16),
            pltpu.VMEM((total, 128), f32),
            pltpu.VMEM((2, depth, width), bf16),
            pltpu.VMEM((2, depth, width), bf16),
            pltpu.VMEM((2, local, piece_rows, width), bf16),
            pltpu.VMEM((local, total, width), bf16),
            pltpu.VMEM((tp - 1, total, quarter), bf16),
            pltpu.VMEM((total, quarter), bf16),
            dma((SLOTS,)),
            dma((steps, fs)), dma((steps, fs)),
            dma((steps, fs, gr - 1)), dma((steps, fs, gr - 1)),
            dma((steps,)),
            dma((fs,)), dma((fs,)), dma((fs,)), dma((fs,)),
            dma((fs, tp)), dma((fs, tp)),
            dma((2,)),
            dma((2, 2)), dma((2,)),
            dma((tp * per_owner,)), dma((tp - 1, per_owner)),
            dma((fs,)), dma((fs,)), dma((2,)),
        ],
        compiler_params=pltpu.CompilerParams(
            collective_id=0, has_side_effects=True, vmem_limit_bytes=66000000
        ),
    )(norm_gain[:, None], gate_master, up_master, down_master, packed, sent_w)
    answers = answers.reshape(groups, fs // groups, cap, quarter)
    answers = jnp.sum(answers.astype(f32), axis=1).astype(bf16).reshape(groups * cap, quarter)
    back = (slot[:, None] == jnp.arange(groups * cap, dtype=jnp.int32)[None, :]).astype(bf16)
    blended = jnp.dot(back, answers, preferred_element_type=f32)
    return (gate_ready, up_ready, down_ready, blended.astype(bf16))


def solution(mesh):
    both = ("gr", "fs")
    in_specs = (
        P(both, None),
        P(both),
        P(None, both, "tp"),
        P(None, both, "tp"),
        P(None, both, "tp"),
        P(both, None),
        P(both, None),
    )
    out_specs = (
        P("fs", None, "tp"),
        P("fs", None, "tp"),
        P("fs", None, "tp"),
        P(both, "tp"),
    )
    return jax.shard_map(
        per_device, mesh=mesh, in_specs=in_specs, out_specs=out_specs, check_vma=False
    )
```

time: 693 us -> 455 us (0.66)
  waiting for transfers between devices: 427 us -> 0 us
  Pallas kernels: 0 us -> 418 us
  blocking collectives: 96.7 us -> 0 us
  local copies, waits for them, and re-layouts: 61.4 us -> 23.6 us
  starting transfers between devices: 30.1 us -> 0 us
  other arithmetic: 33.5 us -> 4.37 us
  matrix products: 25.1 us -> 6.89 us
  between operations: 13.9 us -> 0.7 us
    pallas_call x0 -> x1, Pallas kernels: none -> 418 us  [per_device(): pl.pallas_call(functools.partial(kernel, dims), name='reshard_experts', o...]
    all_to_all x4 -> x0, waiting for transfers between devices: 353 us -> none  [the longest x1 174 us: per_device(): lax.all_to_all(outgoing, 'fs', split_axis=0, concat_axis=0, tiled=True)]
    all_to_all x1 -> x0, blocking collectives: 96.7 us -> none  [per_device(): lax.all_to_all(up_low, 'fs', split_axis=0, concat_axis=1, tiled=True)]
    reduce_scatter x1 -> x0, waiting for transfers between devices: 73.3 us -> none  [per_device(): lax.psum_scatter(partial_value, 'tp', scatter_dimension=3, tiled=True)]
    all_to_all x4 -> x0, starting transfers between devices: 29.8 us -> none  [the longest x1 8.99 us: per_device(): lax.all_to_all(outgoing, 'fs', split_axis=0, concat_axis=0, tiled=True)]
    convert_element_type x4 -> x1, other arithmetic: 19.8 us -> 0.01 us  [per_device(): rank = jnp.sum(jnp.where(hits, counts, 0.0), axis=1).astype(jnp.int32)]
    dot_general x2 -> x4, matrix products: 25.1 us -> 6.89 us  [the longest x1 2.81 us: per_device(): jnp.dot(place.astype(bf16), normed, preferred_element_type=f32).astype(bf16)]
    gather x2 -> x0, local copies, waits for them, and re-layouts: 14.8 us -> none  [the longest x1 10.9 us: per_device(): normed[slot_owner]]
  transfers between devices with their start and end apart: 8 -> 0, of which waited for: 5 -> 0; matrix products, arithmetic and copies ran while one was open for 8% -> 0% of each run, Pallas kernels for 0% -> 0%
where the time goes in v1:
time: 455 us; the launch traced here: 454 us
  Pallas kernels  418 us (92%)
  local copies, waits for them, and re-layouts  23.6 us (5%)
  matrix products  6.89 us (2%)
    pallas_call x1, Pallas kernels, per_device(): pl.pallas_call(functools.partial(kernel, dims), name='reshard_experts', o...  418 us
    unnamed x3, local copies, waits for them, and re-layouts  21.9 us

profile of v1, /device:TPU:20, one launch (start us, length us, event | category | flops | bytes accessed | tf_op | source)
XLA Modules:
  0.0 453.7 jit_solution(3034429766661770995)
XLA Ops:
  0.6 2.1 multiply_reduce_fusion
  2.7 0.7 and_select_fusion
  3.4 0.3 fusion.6
  3.7 0.7 select_reduce_fusion
  4.5 1.5 copy.28.gain
  6.0 1.0 fusion.2
  7.0 0.2 slice_bitcast_fusion.3
  7.2 0.8 pad_maximum_fusion.wsend
  8.1 2.8 fusion.4
  10.9 418.1 %reshard_experts.1 = (bf16[8,2048,256]{2,1,0:T(8,128)(2,1)}, bf16[8,2048,256]{2,1,0:T(8,128)(2,1)}, bf16[8,2048,256]{2,1,0:T(8,128)(2,1)}, bf16[4,256,512]{2,1,0:T(8,128)(2,1)}) custom-call(f32[256,1]{1,0:T(8,128)} %copy.28.gain, f32[32,256,256]{2,1,0:T(8,128)} %gm.1, f32[32,256,256]{2,1,0:T(8,128)} %um.1, f32[32,256,256]{2,1,0:T(8,128)} %dm.1, ...), custom_call_target="tpu_custom_call" | custom-call | tf_op jit(solution)/shard_map/reshard_experts/pallas_call | solution.py:371
  429.0 2.8 fusion.5
  431.8 7.3 %copy.33 = bf16[8,2048,256]{2,1,0:T(8,128)(2,1)} copy(bf16[8,2048,256]{2,1,0:T(8,128)(2,1)} %get-tuple-element.26) | data formatting | bytes 16777216
  439.1 7.3 %copy.34 = bf16[8,2048,256]{2,1,0:T(8,128)(2,1)} copy(bf16[8,2048,256]{2,1,0:T(8,128)(2,1)} %get-tuple-element.27) | data formatting | bytes 16777216
  446.4 7.3 %copy.35 = bf16[8,2048,256]{2,1,0:T(8,128)(2,1)} copy(bf16[8,2048,256]{2,1,0:T(8,128)(2,1)} %get-tuple-element.28) | data formatting | bytes 16777216
  (7 shorter events, 0.1 us)

commit v2 on v1

--- a/solution.py
+++ b/solution.py
@@ -69,9 +69,20 @@
         ]
 
     def w_block(f):
-        return w.at[pl.ds(pl.multiple_of(f * cap, cap), cap), :]
-
-    items = [(s, k) for s in range(len(STEPS)) for k in range(fs)]
+        return w.at[:, pl.ds(pl.multiple_of(f * cap, cap), cap)]
+
+    if fs == 4:
+        odd, side = lax.rem(me_f, 2), lax.rem(me_t, 2)
+        near, far = 1 + 2 * odd, 3 - 2 * odd
+        sending = [
+            jnp.where(side == 0, 2, near), jnp.where(side == 0, far, 2), jnp.where(side == 0, near, far)
+        ]
+        hearing = [2, 1, 3]
+    else:
+        sending = list(range(1, fs))
+        hearing = sending
+    items = [(s, k) for s in range(4) for k in [0] + sending]
+    items += [(s, k) for k in [0] + sending for s in (4, 5)]
 
     def load(i):
         s, k = items[i]
@@ -124,7 +135,7 @@
         lax.fori_loop(0, half, cast, 0)
         if i + SLOTS < len(items):
             load(i + SLOTS).start()
-        if k == 0:
+        if isinstance(k, int) and k == 0:
             c = pltpu.make_async_copy(wb.at[s, 0], region(s, me_g, me_f), own_sem.at[s])
             c.start()
             own_copies[s] = c
@@ -191,7 +202,7 @@
                 xs = x[at, :]
                 pre_gate = jnp.dot(xs, gb[slot], preferred_element_type=jnp.float32) * depth ** (-0.5)
                 pre_up = jnp.dot(xs, ub[slot], preferred_element_type=jnp.float32) * depth ** (-0.5)
-                ws = w[at, :]
+                ws = jnp.transpose(w[:, at])
                 lane = lax.broadcasted_iota(jnp.int32, ws.shape, 1)
                 weight = jnp.sum(jnp.where(lane == e, ws, 0.0), axis=1, keepdims=True)
                 value = pre_gate / (1.0 + jnp.exp(-pre_gate)) * pre_up * weight
@@ -236,6 +247,47 @@
         def _():
             partial_copy(ci).start()
 
+        if ci >= 2:
+            finish(ci - 2)
+
+    def answer_part(p):
+        return pl.ds(pl.multiple_of(p * piece_rows, piece_rows), piece_rows)
+
+    def answer_copy(k, p):
+        f = fs_at(k)
+        at = pl.ds(pl.multiple_of(f * cap, cap), cap)
+        return remote(
+            ys.at[at, answer_part(p)], ans.at[me_f, :, answer_part(p)],
+            rs.at[k, p], rr.at[k, p], {"fs": f},
+        )
+
+    def own_answer(p):
+        at = pl.ds(pl.multiple_of(me_f * cap, cap), cap)
+        return pltpu.make_async_copy(
+            ys.at[at, answer_part(p)], ans.at[me_f, :, answer_part(p)], rl_sem.at[p]
+        )
+
+    def finish(ci):
+        here, owner, p, slot_of, away = chunks[ci]
+
+        @pl.when(jnp.logical_not(away))
+        def _():
+            for j in range(1, tp):
+                ref = yr.at[j - 1, :, answer_part(p)]
+                remote(
+                    ref, ref, ps.at[ci], pr.at[j - 1, p], {"tp": lax.rem(me_t + j, tp)}
+                ).wait_recv()
+            for k in list(range(1, fs)) + [0]:
+                at = pl.ds(pl.multiple_of(fs_at(k) * cap, cap), cap)
+                value = x[at, pl.ds(here, piece_rows)].astype(jnp.float32)
+                for j in range(tp - 1):
+                    value += yr[j, at, answer_part(p)].astype(jnp.float32)
+                ys[at, answer_part(p)] = value.astype(jnp.bfloat16)
+                if k > 0:
+                    answer_copy(k, p).start()
+                else:
+                    own_answer(p).start()
+
     def partial_copy(ci):
         at, owner, piece, slot_of, away = chunks[ci]
         return remote(
@@ -245,7 +297,7 @@
         )
 
     for s in (0, 1, 2):
-        for k in range(1, fs):
+        for k in hearing:
             forward(s, k)
     send_gr(4, 0, wb.at[4, 0])
     for k in range(fs):
@@ -258,7 +310,7 @@
         for k in range(fs):
             arrived_gr(s, k)
     experts_of(0)
-    for k in range(1, fs):
+    for k in hearing:
         forward(3, k)
     send_gr(5, 0, wb.at[5, 0])
     for s in (2, 3):
@@ -271,47 +323,38 @@
     own_copies[4].wait()
     own_copies[5].wait()
     apart = rows == piece_rows
+
+    def others(k):
+        arrived_gr(4, k)
+        arrived_gr(5, k)
+        if apart:
+            for j in range(1, gr):
+                chunk(lax.rem(me_g + gr - j, gr) * fs + fs_from(k))
+
     if apart:
         chunk(me_g * fs + me_f)
-    for k in range(1, fs):
+    last = 0
+    for k in hearing:
         forward(4, k)
         forward(5, k)
         if apart:
             chunk(me_g * fs + fs_from(k))
-    for k in range(fs):
-        arrived_gr(4, k)
-        arrived_gr(5, k)
-        for j in range(1, gr):
-            if apart:
-                chunk(lax.rem(me_g + gr - j, gr) * fs + fs_from(k))
+        others(last)
+        last = k
+    others(last)
     if not apart:
         for index in range(depth // piece_rows):
             chunk(jnp.int32(index))
 
-    for j in range(1, tp):
-        for p in range(per_owner):
-            ref = yr.at[j - 1, :, pl.ds(p * piece_rows, piece_rows)]
-            remote(
-                ref, ref, rl_sem.at[1], pr.at[j - 1, p], {"tp": lax.rem(me_t + j, tp)}
-            ).wait_recv()
-    for k in list(range(1, fs)) + [0]:
-        f = fs_at(k)
-        at = pl.ds(pl.multiple_of(f * cap, cap), cap)
-        value = x[at, pl.ds(pl.multiple_of(me_t * quarter, quarter), quarter)].astype(jnp.float32)
-        for j in range(tp - 1):
-            value += yr[j, at, :].astype(jnp.float32)
-        ys[at, :] = value.astype(jnp.bfloat16)
-        if k > 0:
-            c = remote(ys.at[at, :], ans.at[me_f], rs.at[k], rr.at[k], {"fs": f})
-            c.start()
-            sends.append(c)
-        else:
-            own_ans = pltpu.make_async_copy(ys.at[at, :], ans.at[me_f], rl_sem.at[0])
-            own_ans.start()
-    for k in range(1, fs):
-        f = fs_from(k)
-        remote(ans.at[f], ans.at[f], rs.at[k], rr.at[k], {"fs": f}).wait_recv()
-    own_ans.wait()
+    for ci in range(max(0, len(chunks) - 2), len(chunks)):
+        finish(ci)
+    for p in range(per_owner):
+        for k in range(1, fs):
+            answer_copy(k, p).wait_send()
+            f = fs_from(k)
+            ref = ans.at[f, :, pl.ds(p * piece_rows, piece_rows)]
+            remote(ref, ref, rs.at[k, p], rr.at[k, p], {"fs": f}).wait_recv()
+        own_answer(p).wait()
     for c in sends:
         c.wait_send()
     for ci in range(len(chunks)):
@@ -358,8 +401,8 @@
         [
             jnp.pad(
                 packed_w[(d * local) // GROUP, :, d * local : (d + 1) * local],
-                ((0, 0), (0, 128 - local)),
-            )
+                ((0, 0), (0, max(8, local) - local)),
+            ).T
             for d in range(fs)
         ]
     )
@@ -378,7 +421,7 @@
             pltpu.VMEM((SLOTS, half, rows, width), f32),
             pltpu.VMEM((steps, fs, half, rows, width), bf16),
             pltpu.VMEM((total, depth), bf16),
-            pltpu.VMEM((total, 128), f32),
+            pltpu.VMEM((max(8, local), total), f32),
             pltpu.VMEM((2, depth, width), bf16),
             pltpu.VMEM((2, depth, width), bf16),
             pltpu.VMEM((2, local, piece_rows, width), bf16),
@@ -394,7 +437,7 @@
             dma((2,)),
             dma((2, 2)), dma((2,)),
             dma((tp * per_owner,)), dma((tp - 1, per_owner)),
-            dma((fs,)), dma((fs,)), dma((2,)),
+            dma((fs, per_owner)), dma((fs, per_owner)), dma((per_owner,)),
         ],
         compiler_params=pltpu.CompilerParams(
             collective_id=0, has_side_effects=True, vmem_limit_bytes=66000000

time: 455 us -> 437 us (0.960); the launches traced: 454 us -> 431 us
  Pallas kernels: 418 us -> 396 us
    pallas_call x1, Pallas kernels: 418 us -> 396 us  [per_device(): pl.pallas_call(functools.partial(kernel, dims), name='reshard_experts', o...]
    unnamed x3 -> x5, local copies, waits for them, and re-layouts: 21.9 us -> 22 us
where the time goes in v2:
time: 437 us; the launch traced here: 431 us
  Pallas kernels  396 us (91%)
  local copies, waits for them, and re-layouts  22.8 us (5%)
  matrix products  6.96 us (2%)
    pallas_call x1, Pallas kernels, per_device(): pl.pallas_call(functools.partial(kernel, dims), name='reshard_experts', o...  396 us
    unnamed x5, local copies, waits for them, and re-layouts  22 us

profile of v2, /device:TPU:20, one launch (start us, length us, event | category | flops | bytes accessed | tf_op | source)
XLA Modules:
  0.0 430.8 jit_solution(12379699192008056385)
XLA Ops:
  0.6 0.0 copy-start
  0.6 0.7 and_select_fusion
  1.3 0.3 fusion.6
  1.6 0.7 select_reduce_fusion
  2.4 1.1 fusion.2
  3.5 0.6 pad_maximum_fusion.wsend
  4.1 2.1 multiply_reduce_fusion
  6.2 2.8 fusion.4
  9.0 0.0 copy-done
  9.0 0.8 copy.16.gain
  9.8 396.2 %reshard_experts.1 = (bf16[8,2048,256]{2,1,0:T(8,128)(2,1)}, bf16[8,2048,256]{2,1,0:T(8,128)(2,1)}, bf16[8,2048,256]{2,1,0:T(8,128)(2,1)}, bf16[4,256,512]{2,1,0:T(8,128)(2,1)}) custom-call(f32[256,1]{1,0:T(8,128)} %copy.16.gain, f32[32,256,256]{2,1,0:T(8,128)} %gm.1, f32[32,256,256]{2,1,0:T(8,128)} %um.1, f32[32,256,256]{2,1,0:T(8,128)} %dm.1, ...), custom_call_target="tpu_custom_call" | custom-call | tf_op jit(solution)/shard_map/reshard_experts/pallas_call | solution.py:414
  406.1 2.8 fusion.5
  408.9 7.3 %copy.20 = bf16[8,2048,256]{2,1,0:T(8,128)(2,1)} copy(bf16[8,2048,256]{2,1,0:T(8,128)(2,1)} %get-tuple-element.22) | data formatting | bytes 16777216
  416.2 7.3 %copy.21 = bf16[8,2048,256]{2,1,0:T(8,128)(2,1)} copy(bf16[8,2048,256]{2,1,0:T(8,128)(2,1)} %get-tuple-element.23) | data formatting | bytes 16777216
  423.5 7.3 %copy.22 = bf16[8,2048,256]{2,1,0:T(8,128)(2,1)} copy(bf16[8,2048,256]{2,1,0:T(8,128)(2,1)} %get-tuple-element.24) | data formatting | bytes 16777216
  (6 shorter events, 0.0 us)
Async XLA Ops:
  0.6 8.4 %copy-start = (f32[256]{0:T(256)S(1)}, f32[256]{0:T(256)}, u32[]{:S(2)}) copy-start(f32[256]{0:T(256)} %param.8) | copy-start | bytes 3076
